TPU v7x, 32 devices: a whole 2x2x4 slice. The times are simulated.
32 devices in a mesh: sp: 8 (over z, y), tp: 4 (over x, core).
Axes of the slice: x: 2, y: 2, z: 4, core: 2. Of those that a mesh axis runs over, the one named last changes fastest.
Arguments:
- tokens: bfloat16 [6, 2048, 2048], P(None, 'sp', 'tp'), may hold values from -6 to 6
- norm_gains: float32 [3, 2048], replicated, may hold values from 0.5 to 1.5
- weight_outer: bfloat16 [3, 2048, 1024], P(None, 'sp', 'tp'), may hold values from -0.125 to 0.125
- weight_inner: bfloat16 [3, 2048, 1024], P(None, 'sp', 'tp'), may hold values from -0.125 to 0.125
- weight_value: bfloat16 [3, 2048, 1024], P(None, 'sp', 'tp'), may hold values from -0.125 to 0.125
- conv_taps: bfloat16 [3, 3, 1024], P(None, None, 'tp'), may hold values from -3.5 to 3.5
- weight_output: bfloat16 [3, 1024, 2048], P(None, 'sp', 'tp'), may hold values from -0.1875 to 0.1875
Outputs:
- mixed_out: float32 [6, 2048, 2048], P(None, 'sp', 'tp')
All inputs are finite; a program needn't handle non-finite values.
Results may differ from a plain program's by a relative error of at most 0.03.
Values may be sent and summed in bfloat16 or wider, within the bound.
A program may use at most 128 MiB of HBM per device.

v0:
```python
import jax
import jax.numpy as jnp
from jax import lax
from jax.sharding import PartitionSpec as P

epsilon = 1e-06


def taken_in(array, axis, dim, take_in, carry):
    whole = jax.tree.map(lambda part: lax.all_gather(part, axis, axis=dim, tiled=True), array)
    return take_in(carry, whole, jnp.int32(0))


def from_behind(block, axis, distance):
    devices = range(lax.axis_size(axis))
    route = [(i - distance, i) for i in devices if i - distance in devices]
    return lax.ppermute(block, axis, route)


def normalize(values_in, gain_row):
    values = values_in.astype(jnp.float32)
    scale = lax.rsqrt(jnp.mean(values * values, axis=-1, keepdims=True) + epsilon)
    return (values * scale * gain_row.astype(jnp.float32)).astype(jnp.bfloat16)


def convolve(extended, taps):
    width = taps.shape[0]
    out_rows = extended.shape[1] - (width - 1)
    total = jnp.zeros((extended.shape[0], out_rows, extended.shape[2]), jnp.float32)
    for offset in range(width):
        total = total + taps[offset].astype(jnp.float32) * extended[:, offset : offset + out_rows]
    return total


def project_input(normed, pieces_in):
    empty = jnp.zeros((normed.shape[0], pieces_in[0].shape[1]), jnp.float32)

    def add_rows(totals, pieces, start):
        columns = lax.dynamic_slice_in_dim(normed, start, pieces[0].shape[0], 1)
        return tuple(
            (
                total + jnp.dot(columns, piece, preferred_element_type=jnp.float32)
                for total, piece in zip(totals, pieces)
            )
        )

    return taken_in(
        (pieces_in[0], pieces_in[1], pieces_in[2]), "sp", 0, add_rows, (empty, empty, empty)
    )


def project_output(flat_mix, piece_in):
    empty = jnp.zeros((flat_mix.shape[0], piece_in.shape[1]), jnp.float32)

    def add_rows(total, piece, start):
        columns = lax.dynamic_slice_in_dim(flat_mix, start, piece.shape[0], 1)
        return total + jnp.dot(columns, piece, preferred_element_type=jnp.float32)

    return taken_in(piece_in, "sp", 0, add_rows, empty)


def local(tokens, norm_gains, weight_outer, weight_inner, weight_value, conv_taps, weight_output):
    layers = conv_taps.shape[0]
    history = conv_taps.shape[1] - 1
    sequences = tokens.shape[0]
    current = tokens
    result = None
    for layer in range(layers):
        rows = current.shape[1]
        whole = lax.all_gather(current, "tp", axis=2, tiled=True)
        normed = normalize(whole, norm_gains[layer]).reshape(sequences * rows, whole.shape[2])
        outer, inner, value = project_input(
            normed, (weight_outer[layer], weight_inner[layer], weight_value[layer])
        )
        outer = outer.astype(jnp.bfloat16)
        inner = inner.astype(jnp.bfloat16)
        value = value.astype(jnp.bfloat16)
        outer, inner, value = lax.optimization_barrier((outer, inner, value))
        channels = outer.shape[1]
        outer = outer.reshape(sequences, rows, channels)
        gated = (inner.astype(jnp.float32) * value.astype(jnp.float32)).reshape(
            sequences, rows, channels
        )
        earlier = from_behind(gated[:, rows - history :], "sp", 1)
        extended = jnp.concatenate([earlier, gated], axis=1)
        kept = outer
        conved = convolve(extended, conv_taps[layer])
        mixer = (kept.astype(jnp.float32) * conved).astype(jnp.bfloat16)
        out_rows = mixer.shape[1]
        full_mix = lax.all_gather(mixer, "tp", axis=2, tiled=True)
        flat_mix = full_mix.reshape(sequences * out_rows, full_mix.shape[2])
        projected = project_output(flat_mix, weight_output[layer])
        result = projected.reshape(sequences, out_rows, projected.shape[1])
        current = result.astype(jnp.bfloat16)
    return result


def solution(mesh):
    placed = (
        P(None, "sp", "tp"),
        P(),
        P(None, "sp", "tp"),
        P(None, "sp", "tp"),
        P(None, "sp", "tp"),
        P(None, None, "tp"),
        P(None, "sp", "tp"),
    )
    return jax.shard_map(
        local, mesh=mesh, in_specs=placed, out_specs=P(None, "sp", "tp"), check_vma=False
    )
```

profile of v0, /device:TPU:0, one launch (start us, length us, event | category | flops | bytes accessed | tf_op | source)
XLA Modules:
  0.0 757.6 jit_solution(11629076176349233693)
XLA Ops:
  8.4 0.8 fusion.45
  9.2 0.7 fusion.46
  10.0 0.8 fusion.43
  10.9 47.1 %all-gather.31.cloned.1.call-done = bf16[6,256,2048]{2,1,0:T(8,128)(2,1)} async-done(((bf16[6,256,512]{2,1,0:T(8,128)(2,1)}), bf16[6,256,2048]{2,1,0:T(8,128)(2,1)}) %all-gather.31.cloned.1.call-update) | async-done | bytes 6291472 | tf_op jit(solution)/shard_map/all_gather | solution.py:70
  58.0 4.2 fusion
  62.6 4.2 fusion.2
  66.8 33.7 %all-gather.47.cloned.1.call-done = bf16[1,2048,256]{2,1,0:T(8,128)(2,1)} async-done(((bf16[1,256,256]{2,1,0:T(8,128)(2,1)}), bf16[1,2048,256]{2,1,0:T(8,128)(2,1)}) %all-gather.47.cloned.1.call-update) | async-done | bytes 1048592 | tf_op jit(solution)/shard_map/all_gather | solution.py:10
  100.4 4.8 convolution_convert_fusion.6
  105.3 36.3 %all-gather.45.cloned.1.call-done = bf16[1,2048,256]{2,1,0:T(8,128)(2,1)} async-done(((bf16[1,256,256]{2,1,0:T(8,128)(2,1)}), bf16[1,2048,256]{2,1,0:T(8,128)(2,1)}) %all-gather.45.cloned.1.call-update) | async-done | bytes 1048592 | tf_op jit(solution)/shard_map/all_gather | solution.py:10
  141.6 4.9 convolution_convert_fusion.7
  146.5 36.1 %all-gather.43.cloned.1.call-done = bf16[1,2048,256]{2,1,0:T(8,128)(2,1)} async-done(((bf16[1,256,256]{2,1,0:T(8,128)(2,1)}), bf16[1,2048,256]{2,1,0:T(8,128)(2,1)}) %all-gather.43.cloned.1.call-update) | async-done | bytes 1048592 | tf_op jit(solution)/shard_map/all_gather | solution.py:10
  182.6 4.8 convolution_convert_fusion.8
  187.7 2.5 collective-permute-start
  190.2 1.4 collective-permute-done
  191.5 1.5 fusion.26
  193.1 30.5 %all-gather.49.cloned.1.call-done = bf16[1,1024,512]{2,1,0:T(8,128)(2,1)} async-done(((bf16[1,128,512]{2,1,0:T(8,128)(2,1)}), bf16[1,1024,512]{2,1,0:T(8,128)(2,1)}) %all-gather.49.cloned.1.call-update) | async-done | bytes 1048592 | tf_op jit(solution)/shard_map/all_gather | solution.py:10
  223.6 29.1 %all-gather.33.cloned.1.call-done = bf16[6,256,1024]{2,1,0:T(8,128)(2,1)} async-done(((bf16[6,256,256]{2,1,0:T(8,128)(2,1)}), bf16[6,256,1024]{2,1,0:T(8,128)(2,1)}) %all-gather.33.cloned.1.call-update) | async-done | bytes 3145744 | tf_op jit(solution)/shard_map/all_gather | solution.py:90
  252.7 5.1 convolution_convert_fusion.10
  260.8 43.5 %all-gather.35.cloned.1.call-done = bf16[6,256,2048]{2,1,0:T(8,128)(2,1)} async-done(((bf16[6,256,512]{2,1,0:T(8,128)(2,1)}), bf16[6,256,2048]{2,1,0:T(8,128)(2,1)}) %all-gather.35.cloned.1.call-update) | async-done | bytes 6291472 | tf_op jit(solution)/shard_map/all_gather | solution.py:70
  304.3 4.2 fusion.3
  308.9 4.2 fusion.5
  313.1 33.7 %all-gather.55.cloned.1.call-done = bf16[1,2048,256]{2,1,0:T(8,128)(2,1)} async-done(((bf16[1,256,256]{2,1,0:T(8,128)(2,1)}), bf16[1,2048,256]{2,1,0:T(8,128)(2,1)}) %all-gather.55.cloned.1.call-update) | async-done | bytes 1048592 | tf_op jit(solution)/shard_map/all_gather | solution.py:10
  346.7 4.8 convolution_convert_fusion.3
  351.6 36.3 %all-gather.53.cloned.1.call-done = bf16[1,2048,256]{2,1,0:T(8,128)(2,1)} async-done(((bf16[1,256,256]{2,1,0:T(8,128)(2,1)}), bf16[1,2048,256]{2,1,0:T(8,128)(2,1)}) %all-gather.53.cloned.1.call-update) | async-done | bytes 1048592 | tf_op jit(solution)/shard_map/all_gather | solution.py:10
  387.9 4.8 convolution_convert_fusion.4
  392.7 36.2 %all-gather.51.cloned.1.call-done = bf16[1,2048,256]{2,1,0:T(8,128)(2,1)} async-done(((bf16[1,256,256]{2,1,0:T(8,128)(2,1)}), bf16[1,2048,256]{2,1,0:T(8,128)(2,1)}) %all-gather.51.cloned.1.call-update) | async-done | bytes 1048592 | tf_op jit(solution)/shard_map/all_gather | solution.py:10
  428.9 4.9 convolution_convert_fusion.5
  434.0 2.5 collective-permute-start.1
  436.5 1.4 collective-permute-done.1
  437.9 1.5 fusion.20
  439.4 30.6 %all-gather.57.cloned.1.call-done = bf16[1,1024,512]{2,1,0:T(8,128)(2,1)} async-done(((bf16[1,128,512]{2,1,0:T(8,128)(2,1)}), bf16[1,1024,512]{2,1,0:T(8,128)(2,1)}) %all-gather.57.cloned.1.call-update) | async-done | bytes 1048592 | tf_op jit(solution)/shard_map/all_gather | solution.py:10
  470.0 29.1 %all-gather.37.cloned.1.call-done = bf16[6,256,1024]{2,1,0:T(8,128)(2,1)} async-done(((bf16[6,256,256]{2,1,0:T(8,128)(2,1)}), bf16[6,256,1024]{2,1,0:T(8,128)(2,1)}) %all-gather.37.cloned.1.call-update) | async-done | bytes 3145744 | tf_op jit(solution)/shard_map/all_gather | solution.py:90
  499.1 5.1 convolution_convert_fusion.9
  506.8 43.9 %all-gather.39.cloned.1.call-done = bf16[6,256,2048]{2,1,0:T(8,128)(2,1)} async-done(((bf16[6,256,512]{2,1,0:T(8,128)(2,1)}), bf16[6,256,2048]{2,1,0:T(8,128)(2,1)}) %all-gather.39.cloned.1.call-update) | async-done | bytes 6291472 | tf_op jit(solution)/shard_map/all_gather | solution.py:70
  550.8 4.2 fusion.6
  555.4 4.2 fusion.8
  559.5 33.5 %all-gather.63.cloned.1.call-done = bf16[1,2048,256]{2,1,0:T(8,128)(2,1)} async-done(((bf16[1,256,256]{2,1,0:T(8,128)(2,1)}), bf16[1,2048,256]{2,1,0:T(8,128)(2,1)}) %all-gather.63.cloned.1.call-update) | async-done | bytes 1048592 | tf_op jit(solution)/shard_map/all_gather | solution.py:10
  593.0 4.8 convolution_convert_fusion
  597.9 36.2 %all-gather.61.cloned.1.call-done = bf16[1,2048,256]{2,1,0:T(8,128)(2,1)} async-done(((bf16[1,256,256]{2,1,0:T(8,128)(2,1)}), bf16[1,2048,256]{2,1,0:T(8,128)(2,1)}) %all-gather.61.cloned.1.call-update) | async-done | bytes 1048592 | tf_op jit(solution)/shard_map/all_gather | solution.py:10
  634.0 4.8 convolution_convert_fusion.1
  638.9 36.2 %all-gather.59.cloned.1.call-done = bf16[1,2048,256]{2,1,0:T(8,128)(2,1)} async-done(((bf16[1,256,256]{2,1,0:T(8,128)(2,1)}), bf16[1,2048,256]{2,1,0:T(8,128)(2,1)}) %all-gather.59.cloned.1.call-update) | async-done | bytes 1048592 | tf_op jit(solution)/shard_map/all_gather | solution.py:10
  675.0 4.9 convolution_convert_fusion.2
  680.1 2.5 collective-permute-start.2
  682.6 1.4 collective-permute-done.2
  684.0 1.5 fusion.14
  685.5 30.5 %all-gather.65.cloned.1.call-done = bf16[1,1024,512]{2,1,0:T(8,128)(2,1)} async-done(((bf16[1,128,512]{2,1,0:T(8,128)(2,1)}), bf16[1,1024,512]{2,1,0:T(8,128)(2,1)}) %all-gather.65.cloned.1.call-update) | async-done | bytes 1048592 | tf_op jit(solution)/shard_map/all_gather | solution.py:10
  716.0 29.1 %all-gather.41.cloned.1.call-done = bf16[6,256,1024]{2,1,0:T(8,128)(2,1)} async-done(((bf16[6,256,256]{2,1,0:T(8,128)(2,1)}), bf16[6,256,1024]{2,1,0:T(8,128)(2,1)}) %all-gather.41.cloned.1.call-update) | async-done | bytes 3145744 | tf_op jit(solution)/shard_map/all_gather | solution.py:90
  745.1 5.6 fusion.30
  (66 shorter events, 9.3 us)
Async XLA Ops:
  6.5 1.0 copy-start.3
  6.5 1.8 copy-start.4
  6.5 2.7 copy-start.5
  6.5 51.5 %all-gather.31.cloned.1.call-start = ((), (), s32[]{:S(2)}) async-start(), calls=%async_computation | async-start | bytes 7864320 | tf_op jit(solution)/shard_map/all_gather | solution.py:70
  7.3 2.8 copy-start.6
  7.3 93.2 %all-gather.47.cloned.1.call-start = ((), (), s32[]{:S(2)}) async-start(), calls=%async_computation.8 | async-start | bytes 1179648 | tf_op jit(solution)/shard_map/all_gather | solution.py:10
  8.3 2.6 copy-start.7
  8.3 133.3 %all-gather.45.cloned.1.call-start = ((), (), s32[]{:S(2)}) async-start(), calls=%async_computation.7 | async-start | bytes 1179648 | tf_op jit(solution)/shard_map/all_gather | solution.py:10
  9.1 173.5 %all-gather.43.cloned.1.call-start = ((), (), s32[]{:S(2)}) async-start(), calls=%async_computation.6 | async-start | bytes 1179648 | tf_op jit(solution)/shard_map/all_gather | solution.py:10
  10.0 213.6 %all-gather.49.cloned.1.call-start = ((), (), s32[]{:S(2)}) async-start(), calls=%async_computation.9 | async-start | bytes 1179648 | tf_op jit(solution)/shard_map/all_gather | solution.py:10
  10.8 241.8 %all-gather.33.cloned.1.call-start = ((), (), s32[]{:S(2)}) async-start(), calls=%async_computation.1 | async-start | bytes 3932160 | tf_op jit(solution)/shard_map/all_gather | solution.py:90
  58.0 4.6 copy-start
  187.4 2.7 copy-start.8
  187.7 3.9 collective-permute-start
  193.0 111.3 %all-gather.35.cloned.1.call-start = ((), (), s32[]{:S(2)}) async-start(), calls=%async_computation.2 | async-start | bytes 7864320 | tf_op jit(solution)/shard_map/all_gather | solution.py:70
  257.8 88.9 %all-gather.55.cloned.1.call-start = ((), (), s32[]{:S(2)}) async-start(), calls=%async_computation.12 | async-start | bytes 1179648 | tf_op jit(solution)/shard_map/all_gather | solution.py:10
  258.5 129.3 %all-gather.53.cloned.1.call-start = ((), (), s32[]{:S(2)}) async-start(), calls=%async_computation.11 | async-start | bytes 1179648 | tf_op jit(solution)/shard_map/all_gather | solution.py:10
  259.3 169.6 %all-gather.51.cloned.1.call-start = ((), (), s32[]{:S(2)}) async-start(), calls=%async_computation.10 | async-start | bytes 1179648 | tf_op jit(solution)/shard_map/all_gather | solution.py:10
  259.9 210.2 %all-gather.57.cloned.1.call-start = ((), (), s32[]{:S(2)}) async-start(), calls=%async_computation.13 | async-start | bytes 1179648 | tf_op jit(solution)/shard_map/all_gather | solution.py:10
  260.6 238.5 %all-gather.37.cloned.1.call-start = ((), (), s32[]{:S(2)}) async-start(), calls=%async_computation.3 | async-start | bytes 3932160 | tf_op jit(solution)/shard_map/all_gather | solution.py:90
  304.3 4.6 copy-start.2
  434.0 3.9 collective-permute-start.1
  439.4 111.4 %all-gather.39.cloned.1.call-start = ((), (), s32[]{:S(2)}) async-start(), calls=%async_computation.4 | async-start | bytes 7864320 | tf_op jit(solution)/shard_map/all_gather | solution.py:70
  504.2 88.8 %all-gather.63.cloned.1.call-start = ((), (), s32[]{:S(2)}) async-start(), calls=%async_computation.16 | async-start | bytes 1179648 | tf_op jit(solution)/shard_map/all_gather | solution.py:10
  504.8 129.2 %all-gather.61.cloned.1.call-start = ((), (), s32[]{:S(2)}) async-start(), calls=%async_computation.15 | async-start | bytes 1179648 | tf_op jit(solution)/shard_map/all_gather | solution.py:10
  505.4 169.6 %all-gather.59.cloned.1.call-start = ((), (), s32[]{:S(2)}) async-start(), calls=%async_computation.14 | async-start | bytes 1179648 | tf_op jit(solution)/shard_map/all_gather | solution.py:10
  506.0 210.1 %all-gather.65.cloned.1.call-start = ((), (), s32[]{:S(2)}) async-start(), calls=%async_computation.17 | async-start | bytes 1179648 | tf_op jit(solution)/shard_map/all_gather | solution.py:10
  506.6 238.5 %all-gather.41.cloned.1.call-start = ((), (), s32[]{:S(2)}) async-start(), calls=%async_computation.5 | async-start | bytes 3932160 | tf_op jit(solution)/shard_map/all_gather | solution.py:90
  550.8 4.6 copy-start.1
  680.1 3.9 collective-permute-start.2
Sparse Core Ops, SparseCore 0:
  8.9 49.0 all-gather.30
  60.1 40.2 all-gather.46
  102.6 38.9 all-gather.44
  143.6 38.9 all-gather.42
  184.6 38.9 all-gather.48
  225.0 27.6 all-gather.32
  257.9 46.3 all-gather.34
  306.4 40.2 all-gather.54
  348.9 38.9 all-gather.52
  389.9 38.9 all-gather.50
  431.0 38.9 all-gather.56
  471.5 27.6 all-gather.36
  504.4 46.3 all-gather.38
  552.7 40.2 all-gather.62
  595.0 38.9 all-gather.60
  636.0 38.9 all-gather.58
  677.0 38.9 all-gather.64
  717.4 27.6 all-gather.40
where the time goes:
time: 758 us
  waiting for transfers between devices  641 us (85%)
  matrix products  59.6 us (8%)
  other arithmetic  30.2 us (4%)
  between operations  13.9 us (2%)
  starting transfers between devices  8.51 us (1%)
    all_gather x12, waiting for transfers between devices, taken_in(): lax.all_gather(part, axis, axis=dim, tiled=True)  410 us
    all_gather x3, waiting for transfers between devices, local(): whole = lax.all_gather(current, 'tp', axis=2, tiled=True)  134 us
    all_gather x3, waiting for transfers between devices, local(): full_mix = lax.all_gather(mixer, 'tp', axis=2, tiled=True)  87.2 us
    dot_general x9, matrix products, add_rows(): jnp.dot(columns, piece, preferred_element_type=jnp.float32)  43.7 us
    dot_general x3, matrix products, add_rows(): return total + jnp.dot(columns, piece, preferred_element_type=jnp.float32)  15.9 us
  transfers between devices with their start and end apart: 21, of which 21 were waited for; matrix products, arithmetic and copies ran while one was open for 10% of the time, Pallas kernels for 0%

commit v1 on v0

--- a/solution.py
+++ b/solution.py
@@ -67,7 +67,15 @@
     result = None
     for layer in range(layers):
         rows = current.shape[1]
-        whole = lax.all_gather(current, "tp", axis=2, tiled=True)
+        devices_2 = lax.axis_size("tp")
+        current_2, blocks = (current, [current])
+        for _ in range(devices_2 - 1):
+            current_2 = lax.ppermute(
+                current_2, "tp", [(i_2, (i_2 + 1) % devices_2) for i_2 in range(devices_2)]
+            )
+            blocks.insert(0, current_2)
+        line = jnp.concatenate(blocks, axis=2)
+        whole = jnp.roll(line, (lax.axis_index("tp") + 1) * current.shape[2], axis=2)
         normed = normalize(whole, norm_gains[layer]).reshape(sequences * rows, whole.shape[2])
         outer, inner, value = project_input(
             normed, (weight_outer[layer], weight_inner[layer], weight_value[layer])

time: 758 us -> 615 us (0.81); the launches traced: 758 us -> 607 us
  waiting for transfers between devices: 641 us -> 454 us
  other arithmetic: 30.2 us -> 63.9 us
    all_gather x12, waiting for transfers between devices: 410 us -> 189 us  [taken_in(): lax.all_gather(part, axis, axis=dim, tiled=True)]
    ppermute x0 -> x9, waiting for transfers between devices: none -> 172 us  [local(): lax.ppermute(current_2, 'tp', [(i_2, (i_2 + 1) % devices_2) for i_2 in ra...]
    all_gather x3 -> x0, waiting for transfers between devices: 134 us -> none  [local(): whole = lax.all_gather(current, 'tp', axis=2, tiled=True)]
    reduce_sum x3, other arithmetic: 12.7 us -> 46.3 us  [normalize(): jnp.mean(values * values, axis=-1, keepdims=True) + epsilon]
  transfers between devices with their start and end apart: 21 -> 27, of which waited for: 21 -> 22; matrix products, arithmetic and copies ran while one was open for 10% -> 20% of each run, Pallas kernels for 0% -> 0%
where the time goes in v1:
time: 615 us; the launch traced here: 607 us
  waiting for transfers between devices  454 us (74%)
  other arithmetic  63.9 us (10%)
  matrix products  57.3 us (9%)
  between operations  13.9 us (2%)
  starting transfers between devices  9.59 us (2%)
  local copies, waits for them, and re-layouts  8.06 us (1%)
    all_gather x12, waiting for transfers between devices, taken_in(): lax.all_gather(part, axis, axis=dim, tiled=True)  189 us
    ppermute x9, waiting for transfers between devices, local(): lax.ppermute(current_2, 'tp', [(i_2, (i_2 + 1) % devices_2) for i_2 in ra...  172 us
    all_gather x3, waiting for transfers between devices, local(): full_mix = lax.all_gather(mixer, 'tp', axis=2, tiled=True)  87.1 us
    reduce_sum x3, other arithmetic, normalize(): jnp.mean(values * values, axis=-1, keepdims=True) + epsilon  46.3 us
    dot_general x9, matrix products, add_rows(): jnp.dot(columns, piece, preferred_element_type=jnp.float32)  43.7 us
    dot_general x3, matrix products, add_rows(): return total + jnp.dot(columns, piece, preferred_element_type=jnp.float32)  13.6 us
    convert_element_type x3, other arithmetic, normalize(): return (values * scale * gain_row.astype(jnp.float32)).astype(jnp.bfloat16)  12.6 us
  transfers between devices with their start and end apart: 27, of which 22 were waited for; matrix products, arithmetic and copies ran while one was open for 20% of the time, Pallas kernels for 0%

profile of v1, /device:TPU:0, one launch (start us, length us, event | category | flops | bytes accessed | tf_op | source)
XLA Modules:
  0.0 606.9 jit_solution(9144804315271501386)
XLA Ops:
  6.5 1.8 fusion.68
  8.9 1.8 fusion.69
  10.8 18.4 %collective-permute-done = bf16[6,256,512]{2,1,0:T(8,128)(2,1)S(1)} collective-permute-done((bf16[6,256,512]{2,1,0:T(8,128)(2,1)}, bf16[6,256,512]{2,1,0:T(8,128)(2,1)S(1)}, u32[]{:S(2)}, u32[]{:S(2)}) %collective-permute-start) | collective-permute-done | bytes 1572896 | tf_op jit(solution)/shard_map/ppermute | solution.py:73
  29.2 1.8 fusion.70
  31.1 17.9 %collective-permute-done.1 = bf16[6,256,512]{2,1,0:T(8,128)(2,1)S(1)} collective-permute-done((bf16[6,256,512]{2,1,0:T(8,128)(2,1)S(1)}, bf16[6,256,512]{2,1,0:T(8,128)(2,1)S(1)}, u32[]{:S(2)}, u32[]{:S(2)}) %collective-permute-start.1) | collective-permute-done | bytes 1572896 | tf_op jit(solution)/shard_map/ppermute | solution.py:73
  49.0 1.8 fusion.67
  51.8 17.2 %collective-permute-done.2 = bf16[6,256,512]{2,1,0:T(8,128)(2,1)} collective-permute-done((bf16[6,256,512]{2,1,0:T(8,128)(2,1)S(1)}, bf16[6,256,512]{2,1,0:T(8,128)(2,1)}, u32[]{:S(2)}, u32[]{:S(2)}) %collective-permute-start.2) | collective-permute-done | bytes 1572896 | tf_op jit(solution)/shard_map/ppermute | solution.py:73
  68.9 15.0 %fusion = (f32[6,256]{1,0:T(8,128)S(1)}, bf16[6,256,2048]{2,1,0:T(8,128)(2,1)S(1)}) fusion(s32[]{:T(128)S(6)} %select_n.15, bf16[6,256,512]{2,1,0:T(8,128)(2,1)} %param.9, bf16[6,256,512]{2,1,0:T(8,128)(2,1)S(1)} %collective-permute-done, bf16[6,256,512]{2,1,0:T(8,128)(2,1)S(1)} %collective-permute-done.1, bf16[6,256,512]{2,1,0:T(8,128)(2,1)} %collective-permute-done.2), kind=kLoop, calls=%fused_computation.6 | loop fusion | flops 59767296 | bytes 12589060 | tf_op jit(solution)/shard_map/reduce_sum | solution.py:22
  84.0 4.2 fusion.2
  88.1 4.9 convolution_convert_fusion.6
  93.7 4.9 convolution_convert_fusion.7
  98.5 36.3 %all-gather.34.cloned.1.call-done = bf16[1,2048,256]{2,1,0:T(8,128)(2,1)} async-done(((bf16[1,256,256]{2,1,0:T(8,128)(2,1)}), bf16[1,2048,256]{2,1,0:T(8,128)(2,1)}) %all-gather.34.cloned.1.call-update) | async-done | bytes 1048592 | tf_op jit(solution)/shard_map/all_gather | solution.py:10
  134.8 4.8 convolution_convert_fusion.8
  139.9 2.6 collective-permute-start.3
  142.5 1.2 collective-permute-done.3
  143.7 1.5 fusion.47
  145.9 29.9 %all-gather.40.cloned.1.call-done = bf16[1,1024,512]{2,1,0:T(8,128)(2,1)} async-done(((bf16[1,128,512]{2,1,0:T(8,128)(2,1)}), bf16[1,1024,512]{2,1,0:T(8,128)(2,1)}) %all-gather.40.cloned.1.call-update) | async-done | bytes 1048592 | tf_op jit(solution)/shard_map/all_gather | solution.py:10
  175.8 29.0 %all-gather.28.cloned.1.call-done = bf16[6,256,1024]{2,1,0:T(8,128)(2,1)} async-done(((bf16[6,256,256]{2,1,0:T(8,128)(2,1)}), bf16[6,256,1024]{2,1,0:T(8,128)(2,1)}) %all-gather.28.cloned.1.call-update) | async-done | bytes 3145744 | tf_op jit(solution)/shard_map/all_gather | solution.py:98
  204.9 4.0 convolution_convert_fusion.10
  209.2 19.5 %collective-permute-done.4 = bf16[6,256,512]{2,1,0:T(8,128)(2,1)S(1)} collective-permute-done((bf16[6,256,512]{2,1,0:T(8,128)(2,1)S(1)}, bf16[6,256,512]{2,1,0:T(8,128)(2,1)S(1)}, u32[]{:S(2)}, u32[]{:S(2)}) %collective-permute-start.4) | collective-permute-done | bytes 1572896 | tf_op jit(solution)/shard_map/ppermute | solution.py:73
  228.8 19.9 %collective-permute-done.5 = bf16[6,256,512]{2,1,0:T(8,128)(2,1)} collective-permute-done((bf16[6,256,512]{2,1,0:T(8,128)(2,1)S(1)}, bf16[6,256,512]{2,1,0:T(8,128)(2,1)}, u32[]{:S(2)}, u32[]{:S(2)}) %collective-permute-start.5) | collective-permute-done | bytes 1572896 | tf_op jit(solution)/shard_map/ppermute | solution.py:73
  248.8 20.1 %collective-permute-done.6 = bf16[6,256,512]{2,1,0:T(8,128)(2,1)} collective-permute-done((bf16[6,256,512]{2,1,0:T(8,128)(2,1)}, bf16[6,256,512]{2,1,0:T(8,128)(2,1)}, u32[]{:S(2)}, u32[]{:S(2)}) %collective-permute-start.6) | collective-permute-done | bytes 1572896 | tf_op jit(solution)/shard_map/ppermute | solution.py:73
  268.8 15.6 %fusion.3 = (f32[6,256]{1,0:T(8,128)S(1)}, bf16[6,256,2048]{2,1,0:T(8,128)(2,1)S(1)}) fusion(s32[]{:T(128)S(6)} %select_n.15, bf16[6,256,512]{2,1,0:T(8,128)(2,1)S(1)} %convolution_convert_fusion.10, bf16[6,256,512]{2,1,0:T(8,128)(2,1)S(1)} %collective-permute-done.4, bf16[6,256,512]{2,1,0:T(8,128)(2,1)} %collective-permute-done.5, ...), kind=kLoop, calls=%fused_computation.9 | loop fusion | flops 59767296 | bytes 12589060 | tf_op jit(solution)/shard_map/reduce_sum | solution.py:22
  284.5 4.2 fusion.5
  288.7 4.9 convolution_convert_fusion.3
  293.6 4.9 convolution_convert_fusion.4
  298.5 31.0 %all-gather.42.cloned.1.call-done = bf16[1,2048,256]{2,1,0:T(8,128)(2,1)} async-done(((bf16[1,256,256]{2,1,0:T(8,128)(2,1)}), bf16[1,2048,256]{2,1,0:T(8,128)(2,1)}) %all-gather.42.cloned.1.call-update) | async-done | bytes 1048592 | tf_op jit(solution)/shard_map/all_gather | solution.py:10
  329.5 4.8 convolution_convert_fusion.5
  334.5 2.7 collective-permute-start.7
  338.4 1.5 fusion.41
  340.7 29.9 %all-gather.48.cloned.1.call-done = bf16[1,1024,512]{2,1,0:T(8,128)(2,1)} async-done(((bf16[1,128,512]{2,1,0:T(8,128)(2,1)}), bf16[1,1024,512]{2,1,0:T(8,128)(2,1)}) %all-gather.48.cloned.1.call-update) | async-done | bytes 1048592 | tf_op jit(solution)/shard_map/all_gather | solution.py:10
  370.6 29.0 %all-gather.30.cloned.1.call-done = bf16[6,256,1024]{2,1,0:T(8,128)(2,1)} async-done(((bf16[6,256,256]{2,1,0:T(8,128)(2,1)}), bf16[6,256,1024]{2,1,0:T(8,128)(2,1)}) %all-gather.30.cloned.1.call-update) | async-done | bytes 3145744 | tf_op jit(solution)/shard_map/all_gather | solution.py:98
  399.7 4.0 convolution_convert_fusion.9
  404.0 19.5 %collective-permute-done.8 = bf16[6,256,512]{2,1,0:T(8,128)(2,1)S(1)} collective-permute-done((bf16[6,256,512]{2,1,0:T(8,128)(2,1)S(1)}, bf16[6,256,512]{2,1,0:T(8,128)(2,1)S(1)}, u32[]{:S(2)}, u32[]{:S(2)}) %collective-permute-start.8) | collective-permute-done | bytes 1572896 | tf_op jit(solution)/shard_map/ppermute | solution.py:73
  423.6 19.9 %collective-permute-done.9 = bf16[6,256,512]{2,1,0:T(8,128)(2,1)} collective-permute-done((bf16[6,256,512]{2,1,0:T(8,128)(2,1)S(1)}, bf16[6,256,512]{2,1,0:T(8,128)(2,1)}, u32[]{:S(2)}, u32[]{:S(2)}) %collective-permute-start.9) | collective-permute-done | bytes 1572896 | tf_op jit(solution)/shard_map/ppermute | solution.py:73
  443.6 20.1 %collective-permute-done.10 = bf16[6,256,512]{2,1,0:T(8,128)(2,1)} collective-permute-done((bf16[6,256,512]{2,1,0:T(8,128)(2,1)}, bf16[6,256,512]{2,1,0:T(8,128)(2,1)}, u32[]{:S(2)}, u32[]{:S(2)}) %collective-permute-start.10) | collective-permute-done | bytes 1572896 | tf_op jit(solution)/shard_map/ppermute | solution.py:73
  463.7 15.7 %fusion.6 = (f32[6,256]{1,0:T(8,128)S(1)}, bf16[6,256,2048]{2,1,0:T(8,128)(2,1)S(1)}) fusion(s32[]{:T(128)S(6)} %select_n.15, bf16[6,256,512]{2,1,0:T(8,128)(2,1)S(1)} %convolution_convert_fusion.9, bf16[6,256,512]{2,1,0:T(8,128)(2,1)S(1)} %collective-permute-done.8, bf16[6,256,512]{2,1,0:T(8,128)(2,1)} %collective-permute-done.9, ...), kind=kLoop, calls=%fused_computation.12 | loop fusion | flops 59767296 | bytes 12589060 | tf_op jit(solution)/shard_map/reduce_sum | solution.py:22
  479.3 4.2 fusion.8
  483.5 4.9 convolution_convert_fusion
  488.4 4.9 convolution_convert_fusion.1
  493.3 31.0 %all-gather.50.cloned.1.call-done = bf16[1,2048,256]{2,1,0:T(8,128)(2,1)} async-done(((bf16[1,256,256]{2,1,0:T(8,128)(2,1)}), bf16[1,2048,256]{2,1,0:T(8,128)(2,1)}) %all-gather.50.cloned.1.call-update) | async-done | bytes 1048592 | tf_op jit(solution)/shard_map/all_gather | solution.py:10
  524.3 4.8 convolution_convert_fusion.2
  529.3 2.5 collective-permute-start.11
  531.8 1.4 collective-permute-done.11
  533.2 1.5 fusion.35
  534.7 30.6 %all-gather.56.cloned.1.call-done = bf16[1,1024,512]{2,1,0:T(8,128)(2,1)} async-done(((bf16[1,128,512]{2,1,0:T(8,128)(2,1)}), bf16[1,1024,512]{2,1,0:T(8,128)(2,1)}) %all-gather.56.cloned.1.call-update) | async-done | bytes 1048592 | tf_op jit(solution)/shard_map/all_gather | solution.py:10
  565.3 29.0 %all-gather.32.cloned.1.call-done = bf16[6,256,1024]{2,1,0:T(8,128)(2,1)} async-done(((bf16[6,256,256]{2,1,0:T(8,128)(2,1)}), bf16[6,256,1024]{2,1,0:T(8,128)(2,1)}) %all-gather.32.cloned.1.call-update) | async-done | bytes 3145744 | tf_op jit(solution)/shard_map/all_gather | solution.py:98
  594.3 5.6 fusion.51
  (59 shorter events, 6.5 us)
Async XLA Ops:
  6.5 81.6 %all-gather.38.cloned.1.call-start = ((), (), s32[]{:S(2)}) async-start(), calls=%async_computation.5 | async-start | bytes 1179648 | tf_op jit(solution)/shard_map/all_gather | solution.py:10
  8.3 85.3 %all-gather.36.cloned.1.call-start = ((), (), s32[]{:S(2)}) async-start(), calls=%async_computation.4 | async-start | bytes 1179648 | tf_op jit(solution)/shard_map/all_gather | solution.py:10
  8.4 20.8 %collective-permute-start = (bf16[6,256,512]{2,1,0:T(8,128)(2,1)}, bf16[6,256,512]{2,1,0:T(8,128)(2,1)S(1)}, u32[]{:S(2)}, u32[]{:S(2)}) collective-permute-start(bf16[6,256,512]{2,1,0:T(8,128)(2,1)} %param.9), channel_id=1, source_target_pairs={{0,1},{1,2},{2,3},{3,0},{4,5},{5,6},{6,7},{7,4},{8,9},{9,10},{10,1... | collective-permute-start | bytes 4718600 | tf_op jit(solution)/shard_map/ppermute | solution.py:73
  10.7 124.1 %all-gather.34.cloned.1.call-start = ((), (), s32[]{:S(2)}) async-start(), calls=%async_computation.3 | async-start | bytes 1179648 | tf_op jit(solution)/shard_map/all_gather | solution.py:10
  29.2 19.8 %collective-permute-start.1 = (bf16[6,256,512]{2,1,0:T(8,128)(2,1)S(1)}, bf16[6,256,512]{2,1,0:T(8,128)(2,1)S(1)}, u32[]{:S(2)}, u32[]{:S(2)}) collective-permute-start(bf16[6,256,512]{2,1,0:T(8,128)(2,1)S(1)} %collective-permute-done), channel_id=1, source_target_pairs={{0,1},{1,2},{2,3},{3,0},{4,5},{5,6},{6,7},{7,4},{8,9},{9,10},{10,1... | collective-permute-start | bytes 4718600 | tf_op jit(solution)/shard_map/ppermute | solution.py:73
  31.0 144.8 %all-gather.40.cloned.1.call-start = ((), (), s32[]{:S(2)}) async-start(), calls=%async_computation.6 | async-start | bytes 1179648 | tf_op jit(solution)/shard_map/all_gather | solution.py:10
  49.0 19.9 %collective-permute-start.2 = (bf16[6,256,512]{2,1,0:T(8,128)(2,1)S(1)}, bf16[6,256,512]{2,1,0:T(8,128)(2,1)}, u32[]{:S(2)}, u32[]{:S(2)}) collective-permute-start(bf16[6,256,512]{2,1,0:T(8,128)(2,1)S(1)} %collective-permute-done.1), channel_id=1, source_target_pairs={{0,1},{1,2},{2,3},{3,0},{4,5},{5,6},{6,7},{7,4},{8,9},{9,10},{10,1... | collective-permute-start | bytes 4718600 | tf_op jit(solution)/shard_map/ppermute | solution.py:73
  50.8 154.1 %all-gather.28.cloned.1.call-start = ((), (), s32[]{:S(2)}) async-start(), calls=%async_computation | async-start | bytes 3932160 | tf_op jit(solution)/shard_map/all_gather | solution.py:98
  98.5 44.0 %copy-start = (bf16[3,3,256]{2,1,0:T(4,128)(2,1)S(1)}, bf16[3,3,256]{2,1,0:T(4,128)(2,1)}, u32[]{:S(2)}) copy-start(bf16[3,3,256]{2,1,0:T(4,128)(2,1)} %param.14) | copy-start | bytes 13828
  139.9 3.9 collective-permute-start.3
  145.2 143.4 %all-gather.46.cloned.1.call-start = ((), (), s32[]{:S(2)}) async-start(), calls=%async_computation.9 | async-start | bytes 1179648 | tf_op jit(solution)/shard_map/all_gather | solution.py:10
  145.8 147.7 %all-gather.44.cloned.1.call-start = ((), (), s32[]{:S(2)}) async-start(), calls=%async_computation.8 | async-start | bytes 1179648 | tf_op jit(solution)/shard_map/all_gather | solution.py:10
  208.8 19.9 %collective-permute-start.4 = (bf16[6,256,512]{2,1,0:T(8,128)(2,1)S(1)}, bf16[6,256,512]{2,1,0:T(8,128)(2,1)S(1)}, u32[]{:S(2)}, u32[]{:S(2)}) collective-permute-start(bf16[6,256,512]{2,1,0:T(8,128)(2,1)S(1)} %convolution_convert_fusion.10), channel_id=1, source_target_pairs={{0,1},{1,2},{2,3},{3,0},{4,5},{5,6},{6,7},{7,4},{8,9},{9,10},{10,1... | collective-permute-start | bytes 4718600 | tf_op jit(solution)/shard_map/ppermute | solution.py:73
  209.2 120.3 %all-gather.42.cloned.1.call-start = ((), (), s32[]{:S(2)}) async-start(), calls=%async_computation.7 | async-start | bytes 1179648 | tf_op jit(solution)/shard_map/all_gather | solution.py:10
  228.7 19.9 %collective-permute-start.5 = (bf16[6,256,512]{2,1,0:T(8,128)(2,1)S(1)}, bf16[6,256,512]{2,1,0:T(8,128)(2,1)}, u32[]{:S(2)}, u32[]{:S(2)}) collective-permute-start(bf16[6,256,512]{2,1,0:T(8,128)(2,1)S(1)} %collective-permute-done.4), channel_id=1, source_target_pairs={{0,1},{1,2},{2,3},{3,0},{4,5},{5,6},{6,7},{7,4},{8,9},{9,10},{10,1... | collective-permute-start | bytes 4718600 | tf_op jit(solution)/shard_map/ppermute | solution.py:73
  228.8 141.9 %all-gather.48.cloned.1.call-start = ((), (), s32[]{:S(2)}) async-start(), calls=%async_computation.10 | async-start | bytes 1179648 | tf_op jit(solution)/shard_map/all_gather | solution.py:10
  248.7 20.2 %collective-permute-start.6 = (bf16[6,256,512]{2,1,0:T(8,128)(2,1)}, bf16[6,256,512]{2,1,0:T(8,128)(2,1)}, u32[]{:S(2)}, u32[]{:S(2)}) collective-permute-start(bf16[6,256,512]{2,1,0:T(8,128)(2,1)} %collective-permute-done.5), channel_id=1, source_target_pairs={{0,1},{1,2},{2,3},{3,0},{4,5},{5,6},{6,7},{7,4},{8,9},{9,10},{10,1... | collective-permute-start | bytes 4718600 | tf_op jit(solution)/shard_map/ppermute | solution.py:73
  248.7 151.0 %all-gather.30.cloned.1.call-start = ((), (), s32[]{:S(2)}) async-start(), calls=%async_computation.1 | async-start | bytes 3932160 | tf_op jit(solution)/shard_map/all_gather | solution.py:98
  334.5 3.9 collective-permute-start.7
  339.9 143.6 %all-gather.54.cloned.1.call-start = ((), (), s32[]{:S(2)}) async-start(), calls=%async_computation.13 | async-start | bytes 1179648 | tf_op jit(solution)/shard_map/all_gather | solution.py:10
  340.6 147.8 %all-gather.52.cloned.1.call-start = ((), (), s32[]{:S(2)}) async-start(), calls=%async_computation.12 | async-start | bytes 1179648 | tf_op jit(solution)/shard_map/all_gather | solution.py:10
  403.7 19.9 %collective-permute-start.8 = (bf16[6,256,512]{2,1,0:T(8,128)(2,1)S(1)}, bf16[6,256,512]{2,1,0:T(8,128)(2,1)S(1)}, u32[]{:S(2)}, u32[]{:S(2)}) collective-permute-start(bf16[6,256,512]{2,1,0:T(8,128)(2,1)S(1)} %convolution_convert_fusion.9), channel_id=1, source_target_pairs={{0,1},{1,2},{2,3},{3,0},{4,5},{5,6},{6,7},{7,4},{8,9},{9,10},{10,1... | collective-permute-start | bytes 4718600 | tf_op jit(solution)/shard_map/ppermute | solution.py:73
  404.0 120.3 %all-gather.50.cloned.1.call-start = ((), (), s32[]{:S(2)}) async-start(), calls=%async_computation.11 | async-start | bytes 1179648 | tf_op jit(solution)/shard_map/all_gather | solution.py:10
  423.5 19.9 %collective-permute-start.9 = (bf16[6,256,512]{2,1,0:T(8,128)(2,1)S(1)}, bf16[6,256,512]{2,1,0:T(8,128)(2,1)}, u32[]{:S(2)}, u32[]{:S(2)}) collective-permute-start(bf16[6,256,512]{2,1,0:T(8,128)(2,1)S(1)} %collective-permute-done.8), channel_id=1, source_target_pairs={{0,1},{1,2},{2,3},{3,0},{4,5},{5,6},{6,7},{7,4},{8,9},{9,10},{10,1... | collective-permute-start | bytes 4718600 | tf_op jit(solution)/shard_map/ppermute | solution.py:73
  423.6 141.7 %all-gather.56.cloned.1.call-start = ((), (), s32[]{:S(2)}) async-start(), calls=%async_computation.14 | async-start | bytes 1179648 | tf_op jit(solution)/shard_map/all_gather | solution.py:10
  443.5 20.2 %collective-permute-start.10 = (bf16[6,256,512]{2,1,0:T(8,128)(2,1)}, bf16[6,256,512]{2,1,0:T(8,128)(2,1)}, u32[]{:S(2)}, u32[]{:S(2)}) collective-permute-start(bf16[6,256,512]{2,1,0:T(8,128)(2,1)} %collective-permute-done.9), channel_id=1, source_target_pairs={{0,1},{1,2},{2,3},{3,0},{4,5},{5,6},{6,7},{7,4},{8,9},{9,10},{10,1... | collective-permute-start | bytes 4718600 | tf_op jit(solution)/shard_map/ppermute | solution.py:73
  443.5 150.8 %all-gather.32.cloned.1.call-start = ((), (), s32[]{:S(2)}) async-start(), calls=%async_computation.2 | async-start | bytes 3932160 | tf_op jit(solution)/shard_map/all_gather | solution.py:98
  529.3 3.9 collective-permute-start.11
Sparse Core Ops, SparseCore 0:
  9.5 42.9 all-gather.37
  54.6 39.0 all-gather.35
  95.8 38.9 all-gather.33
  136.8 38.9 all-gather.39
  177.2 27.6 all-gather.27
  206.8 40.2 all-gather.45
  249.3 39.0 all-gather.43
  290.5 38.9 all-gather.41
  331.6 38.9 all-gather.47
  372.0 27.6 all-gather.29
  401.8 40.2 all-gather.53
  444.1 39.0 all-gather.51
  485.3 38.9 all-gather.49
  526.3 38.9 all-gather.55
  566.7 27.6 all-gather.31
